TPU v7x, 32 devices: a whole 2x2x4 slice. The times are simulated.
32 devices in a mesh: rep: 2 (over core), fs: 8 (over z, y), tp: 2 (over x).
Axes of the slice: x: 2, y: 2, z: 4, core: 2. Of those that a mesh axis runs over, the one named last changes fastest.
Arguments:
- tokens: bfloat16 [16, 768, 2048], P(('rep', 'fs')), may hold values from -6 to 6
- mixer_gain: float32 [2048], replicated, may hold values from 0.1 to 1.9
- value_weight: float32 [2048, 4, 512], P('fs', None, 'tp'), may hold values from -0.125 to 0.125
- value_scale: float32 [4, 512], P(None, 'tp'), may hold values from 0.5 to 2
- gate_weight: float32 [2048, 4, 512], P('fs', None, 'tp'), may hold values from -0.125 to 0.125
- gate_scale: float32 [4, 512], P(None, 'tp'), may hold values from 0.5 to 2
- pool_weight: float32 [4, 512, 512], P(None, 'fs', 'tp'), may hold values from -0.25 to 0.25
- pool_scale: float32 [4, 512], P(None, 'tp'), may hold values from 0.5 to 2
- channel_gain: float32 [2048], replicated, may hold values from 0.1 to 1.9
- up_weight: float32 [2048, 4096], P('fs', 'tp'), may hold values from -0.125 to 0.125
- up_scale: float32 [4096], P('tp'), may hold values from 0.5 to 2
- down_weight: float32 [4096, 2048], P('tp', 'fs'), may hold values from -0.09375 to 0.09375
- down_scale: float32 [2048], P('fs'), may hold values from 0.5 to 2
Outputs:
- layer_out: bfloat16 [16, 768, 2048], P(('rep', 'fs'), 'tp')
All inputs are finite; a program needn't handle non-finite values.
Results may differ from a plain program's by a relative error of at most 0.015.
Values may be sent and summed in bfloat16 or wider, within the bound.
A program may use at most 64 MiB of HBM per device.

v0:
```python
import functools

import jax
import jax.numpy as jnp
from jax import lax
from jax.experimental import pallas as pl
from jax.experimental.pallas import tpu as pltpu
from jax.sharding import PartitionSpec as P

NY = 2
UP, DOWN, ACROSS, SIBLING = range(4)


class Gather:
    def __init__(self, sizes, srcs, fulls, axes, send_sem, recv_sem, local_sem):
        self.nf = sizes["fs"]
        self.nz = self.nf // NY
        self.rep, self.place, self.tp = lax.axis_index("rep"), lax.axis_index("fs"), lax.axis_index("tp")
        self.z, self.y = self.place // NY, self.place % NY
        self.srcs, self.fulls, self.axes = srcs, fulls, axes
        self.send_sem, self.recv_sem, self.local_sem = send_sem, recv_sem, local_sem

    def target(self, way):
        rep, place = self.rep, self.place
        if way == UP:
            place = place + NY
        elif way == DOWN:
            place = place - NY
        elif way == ACROSS:
            place = self.z * NY + 1 - self.y
        else:
            rep = 1 - rep
        return {"rep": rep, "fs": place, "tp": self.tp}

    def view(self, ref, w, start, size):
        axis = self.axes[w]
        return ref.at[tuple([slice(None)] * axis + [pl.ds(start, size)])]

    def piece(self, w, k, half):
        rows = self.srcs[w].shape[self.axes[w]]
        part = rows // 2
        start = pl.multiple_of(k * rows + half * part, part)
        return self.view(self.fulls[w], w, start, part)

    def copy(self, w, k, way, half=None):
        half = self.rep if half is None else half
        return pltpu.make_async_remote_copy(
            src_ref=self.piece(w, k, half),
            dst_ref=self.piece(w, k, half),
            send_sem=self.send_sem.at[way, w, k],
            recv_sem=self.recv_sem.at[1 if way == SIBLING else 0, w, k],
            device_id=self.target(way),
            device_id_type=pl.DeviceIdType.MESH,
        )

    def barrier(self, others=()):
        sem = pltpu.get_barrier_semaphore()

        def greet(device):
            pl.semaphore_signal(sem, inc=1, device_id=device, device_id_type=pl.DeviceIdType.MESH)

        for way in (ACROSS, SIBLING):
            greet(self.target(way))
        for device in others:
            greet(device)
        pl.when(self.z > 0)(lambda: greet(self.target(DOWN)))
        pl.when(self.z < self.nz - 1)(lambda: greet(self.target(UP)))
        ends = (self.z > 0).astype(jnp.int32) + (self.z < self.nz - 1).astype(jnp.int32)
        pl.semaphore_wait(sem, 2 + len(others) + ends)

    def local(self, w):
        rows = self.srcs[w].shape[self.axes[w]]
        return pltpu.make_async_copy(
            self.srcs[w], self.view(self.fulls[w], w, pl.multiple_of(self.place * rows, rows), rows), self.local_sem.at[w]
        )

    def own(self, w):
        pl.when(self.z < self.nz - 1)(lambda: self.copy(w, self.place, UP).start())
        pl.when(self.z > 0)(lambda: self.copy(w, self.place, DOWN).start())
        self.copy(w, self.place, ACROSS).start()

    def pass_on(self, w, k, ways):
        self.copy(w, k, ACROSS).wait_recv()
        for way in ways:
            if way == UP:
                pl.when(self.z < self.nz - 1)(lambda: self.copy(w, k, UP).start())
            elif way == DOWN:
                pl.when(self.z > 0)(lambda: self.copy(w, k, DOWN).start())
            else:
                self.copy(w, k, way).start()

    def along(self, w, d):
        pl.when(self.z >= d)(lambda: self.pass_on(w, (self.z - d) * NY + self.y, (UP, ACROSS, SIBLING)))
        pl.when(self.z + d < self.nz)(lambda: self.pass_on(w, (self.z + d) * NY + self.y, (DOWN, ACROSS, SIBLING)))

    def across(self, w, d):
        other = 1 - self.y
        pl.when(self.z >= d)(lambda: self.pass_on(w, (self.z - d) * NY + other, (SIBLING,)))
        if d:
            pl.when(self.z + d < self.nz)(lambda: self.pass_on(w, (self.z + d) * NY + other, (SIBLING,)))

    def ready(self, w):
        @pl.loop(0, self.nf)
        def _(k):
            pl.when(k != self.place)(lambda: self.copy(w, k, SIBLING, half=1 - self.rep).wait_recv())

    def nearest(self, i):
        ends = self.nz - 1 - self.z
        short = jnp.minimum(self.z, ends)
        near = self.z - (i + 1) // 2 if i % 2 else self.z + i // 2
        far = jnp.where(self.z < ends, self.z + (i - short), self.z - (i - short))
        return jnp.where(i <= 2 * short, near, far)

    def drain(self):
        for w in range(len(self.srcs)):

            @pl.loop(0, self.nf)
            def _(k):
                z, y = k // NY, k % NY
                mine = y == self.y
                pl.when(mine & (z <= self.z) & (self.z < self.nz - 1))(lambda: self.copy(w, k, UP).wait_send())
                pl.when(mine & (z >= self.z) & (self.z > 0))(lambda: self.copy(w, k, DOWN).wait_send())
                pl.when(mine)(lambda: self.copy(w, k, ACROSS).wait_send())
                pl.when(k != self.place)(lambda: self.copy(w, k, SIBLING).wait_send())


VALUE, GATE, POOL, SCALES, HIDE, SHOW = range(6)
AXES = (0, 0, 1, 0, 0, 0)


def layer_kernel(sizes, *refs):
    count = len(AXES)
    tokens, mixer_gain, value_scale, gate_scale, pool_scale, channel_gain, up_scale = refs[:7]
    srcs, out, fulls = refs[7 : 7 + count], refs[7 + count], refs[8 + count : 8 + 2 * count]
    normed, excess, excess_in, gate, merged, merged_in, hidden, part_out, part_own, part_in = refs[
        8 + 2 * count : 18 + 2 * count
    ]
    send_sem, recv_sem, local_sem, pair_send, pair_recv = refs[18 + 2 * count :]
    g = Gather(sizes, srcs, fulls, AXES, send_sem, recv_sem, local_sem)
    rows, width = tokens.shape
    groups, _, local = excess.shape
    half = rows // 2
    member = g.tp
    partner = {"rep": g.rep, "fs": g.place, "tp": 1 - member}

    def pair_copy(kind, index, source, target):
        return pltpu.make_async_remote_copy(
            src_ref=source.at[index],
            dst_ref=target.at[index],
            send_sem=pair_send.at[kind, index],
            recv_sem=pair_recv.at[kind, index],
            device_id=partner,
            device_id_type=pl.DeviceIdType.MESH,
        )

    def excess_copy(group):
        return pair_copy(0, group, excess, excess_in)

    def merged_copy(group):
        return pair_copy(1, group, merged, merged_in)

    def part_copy(k):
        return pair_copy(2, k, part_out, part_in)

    def norm_in():
        @pl.loop(0, rows // 16)
        def _(i):
            at = pl.ds(pl.multiple_of(i * 16, 16), 16)
            normed[at, :] = norm_rows(tokens[at, :], mixer_gain[...]).astype(jnp.bfloat16)

    def value_piece(group):
        cut = pl.ds(group * local, local)
        value = jnp.dot(normed[...], fulls[VALUE][:, cut], preferred_element_type=jnp.float32) * value_scale[group : group + 1]
        floats = value.astype(jnp.bfloat16).astype(jnp.float32)
        place = lax.broadcasted_iota(jnp.int32, floats.shape, 0)
        running = floats
        for level in range(group + 1):
            shifted = pltpu.roll(running, 2**level, 0)
            running = running + jnp.where(place >= 2**level, shifted, 0.0)
        counts = jnp.minimum(place + 1, 2 ** (group + 1)).astype(jnp.float32)
        excess[group] = (running / counts - floats).astype(jnp.bfloat16)
        excess_copy(group).start()

    def gate_piece(group):
        cut = pl.ds(group * local, local)

        @pl.loop(0, 2)
        def _(i):
            at = pl.ds(pl.multiple_of(i * half, half), half)
            value = jnp.dot(normed[at, :], fulls[GATE][:, cut], preferred_element_type=jnp.float32)
            gate[group, at, :] = jax.nn.sigmoid(value * gate_scale[group : group + 1])

    def pool_piece(group):
        excess_copy(group).wait_recv()
        weight = fulls[POOL].at[group]
        mine = weight[pl.ds(pl.multiple_of(member * local, local), local), :]
        theirs = weight[pl.ds(pl.multiple_of((1 - member) * local, local), local), :]
        pooled = jnp.dot(excess[group], mine, preferred_element_type=jnp.float32) + jnp.dot(
            excess_in[group], theirs, preferred_element_type=jnp.float32
        )
        scale = pool_scale[group : group + 1]
        merged[group] = (gate[group] * (pooled * scale)).astype(jnp.bfloat16)
        merged_copy(group).start()

    def slabs(at):
        for group in range(groups):
            for source, owner in ((merged, member), (merged_in, 1 - member)):
                cut = pl.ds(pl.multiple_of((2 * group + owner) * local, local), local)
                yield cut, tokens[at, cut].astype(jnp.float32) + source[group, at, :].astype(jnp.float32)

    def norm_mid(part, parts):
        if part == 0:
            for group in range(groups):
                merged_copy(group).wait_recv()
        steps = rows // 16 // parts

        @pl.loop(part * steps, (part + 1) * steps)
        def _(i):
            at = pl.ds(pl.multiple_of(i * 16, 16), 16)
            held = list(slabs(at))
            total = sum(jnp.sum(values * values, axis=-1, keepdims=True) for _, values in held)
            factor = lax.rsqrt(total / width + 1e-06)
            for cut, values in held:
                normed[at, cut] = (values * factor * channel_gain[:, cut]).astype(jnp.bfloat16)

    def up_piece(n):
        cut = pl.ds(n * local, local)

        @pl.loop(0, 2)
        def _(i):
            at = pl.ds(pl.multiple_of(i * half, half), half)
            upward = jnp.dot(normed[at, :], fulls[HIDE][:, cut], preferred_element_type=jnp.float32) * up_scale[:, cut]
            hidden[at, cut] = jnp.square(jax.nn.relu(upward)).astype(jnp.bfloat16)

    inner = hidden.shape[1]

    def down_piece(k, first):
        weight = fulls[SHOW][pl.ds(pl.multiple_of(k * inner, inner), inner), :]
        scale = fulls[SCALES][pl.ds(pl.multiple_of(k * 16, 16), 16), :][:1]
        at = pl.ds(pl.multiple_of(first, half), half)
        part = jnp.dot(hidden[at, :], weight, preferred_element_type=jnp.float32) * scale
        return part.astype(jnp.bfloat16)

    def down_step(i, y):
        k = g.nearest(i) * NY + y
        if i or y is not g.y:
            g.copy(SHOW, k, SIBLING, half=1 - g.rep).wait_recv()
        part_out[k] = down_piece(k, (1 - member) * half)
        part_copy(k).start()
        part_own[k] = down_piece(k, member * half)

    def finish():
        wide = fulls[SHOW].shape[1]

        @pl.loop(0, g.nf)
        def _(k):
            part_copy(k).wait_recv()
            cut = pl.ds(pl.multiple_of(k * wide, wide), wide)
            summed = part_own[k].astype(jnp.float32) + part_in[k].astype(jnp.float32)
            out[:, cut] = (middle_of(k) + summed).astype(out.dtype)

    def middle_of(k):
        group, owner = k // 2, k % 2
        cut = pl.ds(pl.multiple_of(k * local, local), local)
        at = pl.ds(pl.multiple_of(member * half, half), half)
        own = merged[group, at, :].astype(jnp.float32)
        other = merged_in[group, at, :].astype(jnp.float32)
        return tokens[at, cut].astype(jnp.float32) + jnp.where(owner == member, own, other)

    work = []

    def emit(n):
        for _ in range(min(n, len(work))):
            work.pop(0)()

    def queue(w):
        g.ready(w)
        if w == VALUE:
            work.extend(functools.partial(value_piece, i) for i in range(groups))
        elif w == GATE:
            work.extend(functools.partial(gate_piece, i) for i in range(groups))
        elif w == SCALES:
            work.extend(functools.partial(pool_piece, i) for i in range(groups))
            work.extend(functools.partial(norm_mid, i, 3) for i in range(3))
        elif w == HIDE:
            work.extend(functools.partial(up_piece, i) for i in range(inner // local))

    other = 1 - g.y
    for w in range(count):
        g.local(w).start()
    g.barrier((partner,))
    for w in range(count):
        g.local(w).wait()
    g.own(0)
    norm_in()
    for w in range(count):
        for d in range(1, g.nz):
            g.along(w, d)
            if d == 1:
                if w + 1 < count:
                    g.own(w + 1)
                if w:
                    g.across(w - 1, g.nz - 1)
                    queue(w - 1)
                    if w == SHOW:
                        work.append(functools.partial(down_step, 0, g.y))
            else:
                g.across(w, d - 2)
            if w == SHOW:
                work.append(functools.partial(down_step, d, g.y))
                if d > 1:
                    work.append(functools.partial(down_step, d - 2, other))
            emit(4 if w == SHOW else 2)
        g.across(w, g.nz - 2)
        if w == SHOW:
            work.append(functools.partial(down_step, g.nz - 2, other))
        emit(4 if w == SHOW else 2)
    emit(len(work))
    g.across(count - 1, g.nz - 1)
    down_step(g.nz - 1, other)
    finish()
    for group in range(groups):
        excess_copy(group).wait_send()
        merged_copy(group).wait_send()

    @pl.loop(0, g.nf)
    def _(k):
        part_copy(k).wait_send()

    g.drain()


def run_layer(sizes, tokens, vectors, weights):
    rows, width = tokens.shape
    count = len(weights)
    fulls = []
    for weight, axis in zip(weights, AXES):
        shape = list(weight.shape)
        shape[axis] *= sizes["fs"]
        fulls.append(pltpu.VMEM(tuple(shape), weight.dtype))
    groups, _, local = weights[POOL].shape
    inner, wide = weights[SHOW].shape
    halves = (sizes["fs"], rows // 2, wide)
    pieces = (groups, rows, local)
    return pl.pallas_call(
        functools.partial(layer_kernel, sizes),
        out_shape=jax.ShapeDtypeStruct((rows // 2, width), jnp.bfloat16),
        in_specs=[pl.BlockSpec(memory_space=pltpu.VMEM)] * (1 + len(vectors))
        + [pl.BlockSpec(memory_space=pl.ANY)] * count,
        out_specs=pl.BlockSpec(memory_space=pltpu.VMEM),
        scratch_shapes=fulls
        + [
            pltpu.VMEM((rows, width), jnp.bfloat16),
            pltpu.VMEM(pieces, jnp.bfloat16),
            pltpu.VMEM(pieces, jnp.bfloat16),
            pltpu.VMEM(pieces, jnp.float32),
            pltpu.VMEM(pieces, jnp.bfloat16),
            pltpu.VMEM(pieces, jnp.bfloat16),
            pltpu.VMEM((rows, inner), jnp.bfloat16),
            pltpu.VMEM(halves, jnp.bfloat16),
            pltpu.VMEM(halves, jnp.bfloat16),
            pltpu.VMEM(halves, jnp.bfloat16),
            pltpu.SemaphoreType.DMA((4, count, sizes["fs"])),
            pltpu.SemaphoreType.DMA((2, count, sizes["fs"])),
            pltpu.SemaphoreType.DMA((count,)),
            pltpu.SemaphoreType.DMA((3, 8)),
            pltpu.SemaphoreType.DMA((3, 8)),
        ],
        compiler_params=pltpu.CompilerParams(
            collective_id=0, has_side_effects=True, vmem_limit_bytes=63 * 2**20
        ),
    )(tokens, *vectors, *weights)


def norm_rows(values, gain):
    floats = values.astype(jnp.float32)
    return floats * lax.rsqrt(jnp.mean(floats * floats, axis=-1, keepdims=True) + 1e-06) * gain


def pool_excess(value):
    floats = value.astype(jnp.float32)
    seq_length = floats.shape[1]
    running = floats
    results = []
    for group in range(floats.shape[2]):
        span = 2**group
        shifted = jnp.pad(running, ((0, 0), (span, 0), (0, 0), (0, 0)))[:, :seq_length]
        running = running + shifted
        counts = jnp.minimum(jnp.arange(1, seq_length + 1), 2 * span).astype(jnp.float32)
        results.append(running[:, :, group, :] / counts[None, :, None] - floats[:, :, group, :])
    return jnp.stack(results, axis=2)


def per_device(
    tokens,
    mixer_gain,
    value_weight,
    value_scale,
    gate_weight,
    gate_scale,
    pool_weight,
    pool_scale,
    channel_gain,
    up_weight,
    up_scale,
    down_weight,
    down_scale,
):
    seq_count, seq_length, model_width = tokens.shape
    shares = lax.axis_size("tp")
    member = lax.axis_index("tp")
    kept_rows = seq_length // shares
    row_count = seq_count * seq_length
    group_count, local_width = value_scale.shape
    value_full, gate_full, pool_full = (
        lax.all_gather(value_weight.astype(jnp.bfloat16), "fs", axis=0, tiled=True),
        lax.all_gather(gate_weight.astype(jnp.bfloat16), "fs", axis=0, tiled=True),
        lax.all_gather(pool_weight.astype(jnp.bfloat16), "fs", axis=1, tiled=True),
    )
    down_scales = lax.all_gather(down_scale, "fs", axis=0, tiled=True)
    normed = norm_rows(tokens, mixer_gain).astype(jnp.bfloat16).reshape(row_count, model_width)
    value = jnp.dot(normed, value_full.reshape(model_width, -1), preferred_element_type=jnp.float32)
    value = (
        (value * value_scale.reshape(-1))
        .astype(jnp.bfloat16)
        .reshape(seq_count, seq_length, group_count, local_width)
    )
    gating = jnp.dot(normed, gate_full.reshape(model_width, -1), preferred_element_type=jnp.float32)
    gating = (gating * gate_scale.reshape(-1)).reshape(
        seq_count, seq_length, group_count, local_width
    )
    excess = pool_excess(value).astype(jnp.bfloat16)
    rows_part = pool_full
    pooled = jnp.einsum(
        "slgc,gce->slge",
        lax.all_gather(excess, "tp", axis=3, tiled=True),
        rows_part,
        preferred_element_type=jnp.float32,
    )
    merged = (jax.nn.sigmoid(gating) * (pooled * pool_scale)).astype(jnp.bfloat16)
    merged_own = lax.all_to_all(merged, "tp", split_axis=1, concat_axis=3, tiled=True)
    own_rows = lax.dynamic_slice_in_dim(tokens, member * kept_rows, kept_rows, 1)
    middle = own_rows.reshape(seq_count * kept_rows, model_width).astype(
        jnp.float32
    ) + merged_own.reshape(seq_count * kept_rows, model_width).astype(jnp.float32)
    normed_two = norm_rows(middle, channel_gain).astype(jnp.bfloat16)
    up_full, down_full = (
        lax.all_gather(up_weight.astype(jnp.bfloat16), "fs", axis=0, tiled=True),
        lax.all_gather(down_weight.astype(jnp.bfloat16), "fs", axis=1, tiled=True),
    )
    upward = (
        jnp.dot(
            lax.all_gather(normed_two, "tp", axis=0, tiled=True),
            up_full,
            preferred_element_type=jnp.float32,
        )
        * up_scale
    )
    hidden = jnp.square(jax.nn.relu(upward)).astype(jnp.bfloat16)
    rows_part = hidden
    summed = lax.psum_scatter(
        (jnp.dot(rows_part, down_full, preferred_element_type=jnp.float32) * down_scales).astype(
            jnp.bfloat16
        ),
        "tp",
        scatter_dimension=0,
        tiled=True,
    ).astype(jnp.float32)
    return (middle + summed).astype(jnp.bfloat16).reshape(seq_count, kept_rows, model_width)


def paired_device(
    sizes,
    tokens,
    mixer_gain,
    value_weight,
    value_scale,
    gate_weight,
    gate_scale,
    pool_weight,
    pool_scale,
    channel_gain,
    up_weight,
    up_scale,
    down_weight,
    down_scale,
):
    rows = value_weight.shape[0]
    row = lambda vector: vector.reshape(1, -1)
    out = run_layer(
        sizes,
        tokens[0],
        (
            row(mixer_gain),
            value_scale,
            gate_scale,
            pool_scale,
            row(channel_gain),
            row(up_scale),
        ),
        (
            value_weight.astype(jnp.bfloat16).reshape(rows, -1),
            gate_weight.astype(jnp.bfloat16).reshape(rows, -1),
            pool_weight.astype(jnp.bfloat16),
            jnp.broadcast_to(row(down_scale), (16, down_scale.shape[0])),
            up_weight.astype(jnp.bfloat16),
            down_weight.astype(jnp.bfloat16),
        ),
    )
    return out[None]


def solution(mesh):
    sizes = dict(mesh.shape)
    paired = sizes["rep"] == 2 and sizes["tp"] == 2 and sizes["fs"] % NY == 0 and sizes["fs"] == 8

    def body(tokens, *rest):
        value_scale, down_scale = rest[2], rest[-1]
        if paired and tokens.shape[0] == 1 and value_scale.shape[1] == down_scale.shape[0]:
            return paired_device(sizes, tokens, *rest)
        return per_device(tokens, *rest)

    return jax.shard_map(
        body,
        mesh=mesh,
        in_specs=(
            P(("rep", "fs"), None, None),
            P(),
            P("fs", None, "tp"),
            P(None, "tp"),
            P("fs", None, "tp"),
            P(None, "tp"),
            P(None, "fs", "tp"),
            P(None, "tp"),
            P(),
            P("fs", "tp"),
            P("tp"),
            P("tp", "fs"),
            P("fs"),
        ),
        out_specs=P(("rep", "fs"), "tp", None),
        check_vma=False,
    )
```

profile of v0, /device:TPU:0, one launch (start us, length us, event | category | flops | bytes accessed | tf_op | source)
XLA Modules:
  0.0 202.8 jit_solution(3157994565317437579)
XLA Ops:
  0.0 0.0 copy-start.2
  0.0 1.4 broadcast_in_dim.8.refs_10_
  1.4 1.6 convert_element_type.17.refs_9_
  3.0 1.4 convert_element_type.15
  4.4 0.0 copy-start
  4.4 0.9 copy.14
  5.3 0.0 copy-done.2
  5.3 0.2 convert_element_type.16
  5.5 0.0 copy-start.1
  5.5 0.9 copy.15
  6.4 0.0 copy-done
  6.4 1.1 convert_element_type.18.refs_11_
  7.5 0.0 copy-done.1
  7.5 1.1 convert_element_type.19.refs_12_
  8.6 191.4 %shard_map.127 = bf16[384,2048]{1,0:T(8,128)(2,1)} custom-call(bf16[768,2048]{1,0:T(8,128)(2,1)} %bitcast.10, f32[1,2048]{1,0:T(1,128)} %bitcast.15, f32[4,256]{1,0:T(4,128)} %refs_2_.1, f32[4,256]{1,0:T(4,128)} %refs_3_.1, f32[4,256]{1,0:T(4,128)} %refs_4_.1, f32[1,2048]{1,0:T(1,128)} %bitcast.16, f32[1,2048]{1,0:T(1,128)} %bitcast.17, ...), custom_call_target="tpu_custom_call" | custom-call | tf_op jit(solution)/shard_map/pallas_call | solution.py:345
  200.1 2.7 %copy.17 = bf16[1,384,2048]{2,1,0:T(8,128)(2,1)} copy(bf16[1,384,2048]{2,1,0:T(8,128)(2,1)} %bitcast.9) | data formatting | bytes 3145728
Async XLA Ops:
  0.0 5.3 %copy-start.2 = (f32[256,4,256]{2,1,0:T(4,128)S(1)}, f32[256,4,256]{2,1,0:T(4,128)}, u32[]{:S(2)}) copy-start(f32[256,4,256]{2,1,0:T(4,128)} %param.17) | copy-start | bytes 3145732
  4.4 2.0 copy-start
  5.5 2.0 copy-start.1
where the time goes:
time: 203 us
  Pallas kernels  191 us (94%)
  local copies, waits for them, and re-layouts  5.9 us (3%)
  other arithmetic  5.39 us (3%)
    pallas_call x1, Pallas kernels, run_layer(): pl.pallas_call(functools.partial(layer_kernel, sizes), out_shape=jax.Shap...  191 us
    unnamed x9, local copies, waits for them, and re-layouts  4.54 us

commit v1 on v0

v1 whole, which is shorter than its diff:
```python
import functools

import jax
import jax.numpy as jnp
from jax import lax
from jax.experimental import pallas as pl
from jax.experimental.pallas import tpu as pltpu
from jax.sharding import PartitionSpec as P

NY = 2
ACROSS, SIBLING = 2, 3


class Gather:
    def __init__(self, sizes, bufs, sems):
        self.nf = sizes["fs"]
        self.nz = self.nf // NY
        self.rep, self.place, self.tp = lax.axis_index("rep"), lax.axis_index("fs"), lax.axis_index("tp")
        self.z, self.y = self.place // NY, self.place % NY
        self.mixed, self.hide, self.show, self.stage = bufs
        self.send_sem, self.recv_sem = sems
        self.nm, self.nh = self.mixed.shape[0], self.hide.shape[0]
        self.subs = 4
        self.count = self.nm + self.nh + self.subs

    def device(self, way):
        rep, place = self.rep, self.place
        if isinstance(way, int) and way == ACROSS:
            place = self.z * NY + 1 - self.y
        elif isinstance(way, int) and way == SIBLING:
            rep = 1 - rep
        else:
            place = place + NY * (2 * way - 1)
        return {"rep": rep, "fs": place, "tp": self.tp}

    def partner(self):
        return {"rep": self.rep, "fs": self.place, "tp": 1 - self.tp}

    def half_of(self, p):
        j, q = p // 2, p % 2
        return 2 * j + (self.tp if q == 0 else 1 - self.tp)

    def piece(self, p, k, half):
        if isinstance(p, int) and p < self.nm:
            part = self.mixed.shape[2] // 2
            return self.mixed.at[self.half_of(p), k, pl.ds(pl.multiple_of(half * part, 16), part), :]
        if isinstance(p, int) and p < self.nm + self.nh:
            part = self.hide.shape[2] // 2
            return self.hide.at[p - self.nm, k, pl.ds(pl.multiple_of(half * part, 16), part), :]
        part = self.show.shape[1] // (2 * self.subs)
        sub = p - self.nm - self.nh
        return self.show.at[k, pl.ds(pl.multiple_of((2 * sub + half) * part, 16), part), :]

    def copy(self, p, k, way, half=None, src=None):
        half = self.rep if half is None else half
        sibling = isinstance(way, int) and way == SIBLING
        return pltpu.make_async_remote_copy(
            src_ref=self.piece(p, k, half) if src is None else src,
            dst_ref=self.piece(p, k, half),
            send_sem=self.send_sem.at[way, p, k],
            recv_sem=self.recv_sem.at[1 if sibling else 0, p, k],
            device_id=self.device(way),
            device_id_type=pl.DeviceIdType.MESH,
        )

    def inside(self, z):
        return (z >= 0) & (z < self.nz)

    def wide(self, p, zs):
        return ((zs == 0) | (zs == self.nz - 1)) & (self.rep == p % 2)

    def greet(self):
        sem = pltpu.get_barrier_semaphore()

        def signal(device):
            pl.semaphore_signal(sem, inc=1, device_id=device, device_id_type=pl.DeviceIdType.MESH)

        signal(self.device(ACROSS))
        signal(self.device(SIBLING))
        signal(self.partner())
        pl.when(self.z > 0)(lambda: signal(self.device(0)))
        pl.when(self.z < self.nz - 1)(lambda: signal(self.device(1)))

    def meet(self):
        ends = (self.z > 0).astype(jnp.int32) + (self.z < self.nz - 1).astype(jnp.int32)
        pl.semaphore_wait(pltpu.get_barrier_semaphore(), 3 + ends)

    def each(self, phase, body):
        if phase < self.nm + self.nh:
            body(phase)
        else:
            pl.loop(0, self.subs)(lambda sub: body(self.nm + self.nh + sub))

    def source(self, p):
        if not (isinstance(p, int) and p < self.nm and p % 2 == 0):
            return None
        part = self.stage.shape[1] // 2
        rows = pl.ds(pl.multiple_of(self.rep * part, 16), part)
        return self.stage.at[2 * self.tp + p // 2, rows, :]

    def own(self, phase):
        def body(p):
            src = self.source(p)

            @pl.loop(0, 2)
            def _(way):
                there = self.inside(self.z + 2 * way - 1)
                pl.when(there)(lambda: self.copy(p, self.place, way, src=src).start())

            self.copy(p, self.place, ACROSS, src=src).start()

        self.each(phase, body)

    def along(self, phase, d):
        @pl.loop(0, 2)
        def _(way):
            step = 2 * way - 1
            zs = self.z - step * d

            @pl.when(self.inside(zs))
            def _():
                k = zs * NY + self.y

                def body(p):
                    self.copy(p, k, ACROSS).wait_recv()
                    pl.when(self.inside(self.z + step))(lambda: self.copy(p, k, way).start())
                    pl.when(jnp.logical_not(self.wide(p, zs)))(lambda: self.copy(p, k, ACROSS).start())
                    self.copy(p, k, SIBLING).start()

                self.each(phase, body)

    def across(self, phase, d):
        if d == 0:
            k = self.z * NY + 1 - self.y
            way = (self.z == 0).astype(jnp.int32)

            def first(p):
                self.copy(p, k, ACROSS).wait_recv()
                pl.when(self.wide(p, self.z))(lambda: self.copy(p, k, way).start())
                self.copy(p, k, SIBLING).start()

            self.each(phase, first)
            return

        @pl.loop(0, 2)
        def _(way):
            step = 2 * way - 1
            zs = self.z - step * d

            @pl.when(self.inside(zs))
            def _():
                k = zs * NY + 1 - self.y

                def body(p):
                    self.copy(p, k, ACROSS).wait_recv()
                    onward = self.wide(p, zs) & self.inside(self.z + step)
                    pl.when(onward)(lambda: self.copy(p, k, way).start())
                    self.copy(p, k, SIBLING).start()

                self.each(phase, body)

    def wait_sibling(self, phase, k):
        self.each(phase, lambda p: self.copy(p, k, SIBLING, half=1 - self.rep).wait_recv())

    def ready(self, phase):
        @pl.loop(0, self.nf)
        def _(k):
            pl.when(k != self.place)(lambda: self.wait_sibling(phase, k))

    def drain(self, phase):
        def body(p):
            src = self.source(p)

            @pl.loop(0, self.nf)
            def _(k):
                zs, mine = k // NY, k % NY == self.y
                wide = self.wide(p, zs)
                here = zs == self.z

                @pl.loop(0, 2)
                def _(way):
                    step = 2 * way - 1
                    away = here | (step * (self.z - zs) > 0)
                    sent = self.inside(self.z + step) & away & (mine | wide)
                    pl.when(sent)(lambda: self.copy(p, k, way).wait_send())

                pl.when(mine & (here | jnp.logical_not(wide)))(lambda: self.copy(p, k, ACROSS).wait_send())
                pl.when(k != self.place)(lambda: self.copy(p, k, SIBLING).wait_send())

        self.each(phase, body)


def layer_kernel(sizes, *refs):
    mixer_gain, value_scale, gate_scale, pool_scale, channel_gain, up_scale, down_scale = refs[:7]
    tokens_far, value_far, gate_far, pool_far, up_far, down_far, out = refs[7:14]
    mixed, hide, show, stage = refs[14:18]
    tokens, value_near, gate_near, pool_near, up_near, down_near = refs[18:24]
    normed, excess, merged, merged_in, hidden, part_out, part_own, part_in = refs[24:32]
    send_sem, recv_sem, load_sem, swap_send, swap_recv, keep_sem, pair_send, pair_recv = refs[32:]
    g = Gather(sizes, (mixed, hide, show, stage), (send_sem, recv_sem))
    rows, width = tokens.shape
    groups, cells, local = pool_near.shape
    depth = value_near.shape[0]
    half = rows // 2
    inner = hidden.shape[1]
    member, rep, place = g.tp, g.rep, g.place
    nm, nh = g.nm, g.nh
    last = nm + nh
    each_group = nm // 2

    loads = [
        pltpu.make_async_copy(far, near, load_sem.at[i])
        for i, (far, near) in enumerate(
            (
                (value_far, value_near),
                (gate_far, gate_near),
                (pool_far, pool_near),
                (tokens_far, tokens),
                (up_far, up_near),
                (down_far, down_near),
            )
        )
    ]

    def remote(source, target, send, recv):
        return pltpu.make_async_remote_copy(
            src_ref=source,
            dst_ref=target,
            send_sem=send,
            recv_sem=recv,
            device_id=g.partner(),
            device_id_type=pl.DeviceIdType.MESH,
        )

    def swap(j, part):
        size = stage.shape[1] // 2
        cut = pl.ds(pl.multiple_of(part * size, 16), size)
        return remote(
            stage.at[2 * (1 - member) + j, cut, :],
            mixed.at[2 * j + member, place, cut, :],
            swap_send.at[j, part],
            swap_recv.at[j, part],
        )

    def keep(j):
        return pltpu.make_async_copy(stage.at[2 * member + j], mixed.at[2 * j + member, place], keep_sem.at[j])

    def merged_copy(slab):
        return remote(merged.at[slab], merged_in.at[slab], pair_send.at[0, slab], pair_recv.at[0, slab])

    def part_copy(k):
        return remote(part_out.at[k], part_in.at[k], pair_send.at[1, k], pair_recv.at[1, k])

    def round_mixed(group):
        stage[group, :depth, :local] = (value_near[:, group, :] * value_scale[group : group + 1]).astype(jnp.bfloat16)
        stage[group, :depth, local:] = (gate_near[:, group, :] * gate_scale[group : group + 1]).astype(jnp.bfloat16)
        for i in range(2):
            chunk = pool_near[group, i * (cells // 2) : (i + 1) * (cells // 2), :] * pool_scale[group : group + 1]
            stage[group, depth:, i * local : (i + 1) * local] = chunk.astype(jnp.bfloat16)

    def round_up(c):
        wide = hide.shape[3]
        cut = slice(c * wide, (c + 1) * wide)
        hide[c, place] = (up_near[:, cut] * up_scale[:, cut]).astype(jnp.bfloat16)

    def round_down(i):
        part = inner // 4
        at = pl.ds(i * part, part)
        show[place, at, :] = (down_near[at, :] * down_scale[...]).astype(jnp.bfloat16)

    def norm_in(part, parts):
        steps = rows // 16 // parts

        @pl.loop(part * steps, (part + 1) * steps)
        def _(i):
            at = pl.ds(pl.multiple_of(i * 16, 16), 16)
            normed[at, :] = norm_rows(tokens[at, :], mixer_gain[...]).astype(jnp.bfloat16)

    def slab_of(j, q):
        return 2 * j + (member if q == 0 else 1 - member)

    def value_piece(j, q):
        slab = slab_of(j, q)
        weight = mixed[slab, :, :depth, :local].reshape(width, local)
        value = jnp.dot(normed[...], weight, preferred_element_type=jnp.float32)
        floats = value.astype(jnp.bfloat16).astype(jnp.float32)
        position = lax.broadcasted_iota(jnp.int32, floats.shape, 0)
        group = each_group * member + j
        running = floats
        for level in range(groups - each_group + j + 1):
            shifted = pltpu.roll(running, 2**level, 0)
            start = jnp.where(level <= group, 2**level, rows)
            running = running + jnp.where(position >= start, shifted, 0.0)
        window = jnp.int32(2)
        for level in range(groups - 1):
            window = jnp.where(group > level, 2 ** (level + 2), window)
        counts = jnp.minimum(position + 1, window).astype(jnp.float32)
        excess[slab - 2 * j] = (running / counts - floats).astype(jnp.bfloat16)

    def gate_piece(j, q):
        slab = slab_of(j, q)
        gate_weight = mixed[slab, :, :depth, local:].reshape(width, local)
        chunks = [mixed[slab, :, depth:, i * local : (i + 1) * local] for i in range(2)]
        pool = jnp.concatenate(chunks, axis=1).reshape(2 * local, local)

        @pl.loop(0, 2)
        def _(i):
            at = pl.ds(pl.multiple_of(i * half, half), half)
            gate = jnp.dot(normed[at, :], gate_weight, preferred_element_type=jnp.float32)
            pooled = jnp.dot(excess[0, at, :], pool[:local], preferred_element_type=jnp.float32) + jnp.dot(
                excess[1, at, :], pool[local:], preferred_element_type=jnp.float32
            )
            merged[slab, at, :] = (jax.nn.sigmoid(gate) * pooled).astype(jnp.bfloat16)

        merged_copy(slab).start()

    def norm_mid(part, parts):
        if part == 0:
            for slab in range(nm):
                merged_copy(slab).wait_recv()
        steps = rows // 16 // parts

        @pl.loop(part * steps, (part + 1) * steps)
        def _(i):
            at = pl.ds(pl.multiple_of(i * 16, 16), 16)
            held = []
            for slab in range(nm):
                for source, owner in ((merged, member), (merged_in, 1 - member)):
                    cut = pl.ds(pl.multiple_of((nm * owner + slab) * local, local), local)
                    held.append((cut, tokens[at, cut].astype(jnp.float32) + source[slab, at, :].astype(jnp.float32)))
            total = sum(jnp.sum(values * values, axis=-1, keepdims=True) for _, values in held)
            factor = lax.rsqrt(total / width + 1e-06)
            for cut, values in held:
                normed[at, cut] = (values * factor * channel_gain[:, cut]).astype(jnp.bfloat16)

    def up_piece(c, i):
        weight = hide[c, :, :, i * local : (i + 1) * local].reshape(width, local)
        first = c * hide.shape[3] + i * local

        @pl.loop(0, 2)
        def _(b):
            at = pl.ds(pl.multiple_of(b * half, half), half)
            upward = jnp.dot(normed[at, :], weight, preferred_element_type=jnp.float32)
            hidden[at, first : first + local] = jnp.square(jax.nn.relu(upward)).astype(jnp.bfloat16)

    def down_half(k, first):
        at = pl.ds(pl.multiple_of(first, half), half)
        return jnp.dot(hidden[at, :], show[k], preferred_element_type=jnp.float32).astype(jnp.bfloat16)

    def down_step(k):
        part_out[k] = down_half(k, (1 - member) * half)
        part_copy(k).start()
        part_own[k] = down_half(k, member * half)

    def down_at(d, column):
        if d == 0:
            k = g.z * NY + column
            if column is not g.y:
                g.wait_sibling(last, k)
            down_step(k)
            return

        @pl.loop(0, 2)
        def _(way):
            zs = g.z - (2 * way - 1) * d

            @pl.when(g.inside(zs))
            def _():
                k = zs * NY + column
                g.wait_sibling(last, k)
                down_step(k)

    def finish():
        wide = show.shape[2]

        @pl.loop(0, g.nf)
        def _(k):
            part_copy(k).wait_recv()
            cut = pl.ds(pl.multiple_of(k * wide, wide), wide)
            summed = part_own[k].astype(jnp.float32) + part_in[k].astype(jnp.float32)
            out[:, cut] = (middle_of(k) + summed).astype(out.dtype)

    def middle_of(k):
        owner, slab = k // nm, k % nm
        cut = pl.ds(pl.multiple_of(k * local, local), local)
        at = pl.ds(pl.multiple_of(member * half, half), half)
        own = merged[slab, at, :].astype(jnp.float32)
        theirs = merged_in[slab, at, :].astype(jnp.float32)
        return tokens[at, cut].astype(jnp.float32) + jnp.where(owner == member, own, theirs)

    work = []

    def emit(n):
        for _ in range(min(n, len(work))):
            work.pop(0)()

    def add(function, *args):
        work.append(functools.partial(function, *args))

    g.greet()
    for load in loads:
        load.start()
    for load in loads[:3]:
        load.wait()
    for group in range(groups):
        round_mixed(group)
    g.meet()
    swap(0, rep).start()
    g.own(0)
    keep(0).start()
    swap(1, rep).start()
    keep(1).start()
    swap(0, 1 - rep).start()
    swap(1, 1 - rep).start()
    loads[3].wait()
    for i in range(4):
        add(norm_in, i, 4)
    for load in loads[4:]:
        add(load.wait)
    for c in range(nh):
        add(round_up, c)
    for i in range(4):
        add(round_down, i)
    other, pending = 1 - g.y, []
    for phase in range(last + 1):
        g.along(phase, 1)
        g.across(phase, 0)
        if phase + 1 <= last:
            follow = phase + 1
            if follow < nm and follow % 2 == 1:
                swap(follow // 2, rep).wait_recv()
            g.own(follow)
        if phase:
            if phase - 1 < nm and phase % 2 == 0:
                j = (phase - 1) // 2
                keep(j).wait()
                swap(j, 1 - rep).wait_recv()
                g.ready(phase - 2)
                g.ready(phase - 1)
                for q in range(2):
                    add(value_piece, j, q)
                for q in range(2):
                    add(gate_piece, j, q)
            if phase == last - 2:
                for i in range(4):
                    add(norm_mid, i, 4)
            if phase > nm:
                g.ready(phase - 1)
                pending.append(phase - 1 - nm)
            while phase >= last - 2 and pending:
                c = pending.pop(0)
                for i in range(hide.shape[3] // local):
                    add(up_piece, c, i)
        if phase >= 2:
            add(g.drain, phase - 2)
        if phase == last:
            add(down_at, 0, g.y)
            add(down_at, 0, other)
            add(down_at, 1, g.y)
        emit(2)
        for d in range(2, g.nz):
            g.along(phase, d)
            g.across(phase, d - 1)
            if phase == last:
                add(down_at, d, g.y)
                add(down_at, d - 1, other)
            emit(3)
        if phase == last:
            add(g.drain, last - 1)
        g.across(phase, g.nz - 1)
        emit(3)
    emit(len(work))
    down_at(g.nz - 1, other)
    for j in range(2):
        for part in range(2):
            swap(j, part).wait_send()
    for slab in range(nm):
        merged_copy(slab).wait_send()
    g.drain(last)
    finish()

    @pl.loop(0, g.nf)
    def _(k):
        part_copy(k).wait_send()


def run_layer(sizes, vectors, arrays):
    tokens, value, gate, pool, up, down = arrays
    rows, width = tokens.shape
    depth, groups, local = value.shape
    cells = pool.shape[1]
    inner, wide = down.shape
    nf = sizes["fs"]
    vmem = lambda dims, kind=jnp.bfloat16: pltpu.VMEM(tuple(dims), kind)
    halves = (nf, rows // 2, wide)
    count = 12
    return pl.pallas_call(
        functools.partial(layer_kernel, sizes),
        out_shape=jax.ShapeDtypeStruct((rows // 2, width), jnp.bfloat16),
        in_specs=[pl.BlockSpec(memory_space=pltpu.VMEM)] * len(vectors)
        + [pl.BlockSpec(memory_space=pl.ANY)] * len(arrays),
        out_specs=pl.BlockSpec(memory_space=pltpu.VMEM),
        scratch_shapes=[
            vmem((groups, nf, depth + cells // 2, 2 * local)),
            vmem((inner // (2 * local), nf, depth, 2 * local)),
            vmem((nf, inner, wide)),
            vmem((groups, depth + cells // 2, 2 * local)),
            vmem(tokens.shape),
        ]
        + [vmem(array.shape, array.dtype) for array in arrays[1:]]
        + [
            vmem((rows, width)),
            vmem((2, rows, local)),
            vmem((groups, rows, local)),
            vmem((groups, rows, local)),
            vmem((rows, inner)),
            vmem(halves),
            vmem(halves),
            vmem(halves),
            pltpu.SemaphoreType.DMA((4, count, nf)),
            pltpu.SemaphoreType.DMA((2, count, nf)),
            pltpu.SemaphoreType.DMA((len(arrays),)),
            pltpu.SemaphoreType.DMA((2, 2)),
            pltpu.SemaphoreType.DMA((2, 2)),
            pltpu.SemaphoreType.DMA((2,)),
            pltpu.SemaphoreType.DMA((2, nf)),
            pltpu.SemaphoreType.DMA((2, nf)),
        ],
        compiler_params=pltpu.CompilerParams(
            collective_id=0, has_side_effects=True, vmem_limit_bytes=63 * 2**20
        ),
    )(*vectors, *arrays)


def norm_rows(values, gain):
    floats = values.astype(jnp.float32)
    return floats * lax.rsqrt(jnp.mean(floats * floats, axis=-1, keepdims=True) + 1e-06) * gain


def pool_excess(value):
    floats = value.astype(jnp.float32)
    seq_length = floats.shape[1]
    running = floats
    results = []
    for group in range(floats.shape[2]):
        span = 2**group
        shifted = jnp.pad(running, ((0, 0), (span, 0), (0, 0), (0, 0)))[:, :seq_length]
        running = running + shifted
        counts = jnp.minimum(jnp.arange(1, seq_length + 1), 2 * span).astype(jnp.float32)
        results.append(running[:, :, group, :] / counts[None, :, None] - floats[:, :, group, :])
    return jnp.stack(results, axis=2)


def per_device(
    tokens,
    mixer_gain,
    value_weight,
    value_scale,
    gate_weight,
    gate_scale,
    pool_weight,
    pool_scale,
    channel_gain,
    up_weight,
    up_scale,
    down_weight,
    down_scale,
):
    seq_count, seq_length, model_width = tokens.shape
    shares = lax.axis_size("tp")
    member = lax.axis_index("tp")
    kept_rows = seq_length // shares
    row_count = seq_count * seq_length
    group_count, local_width = value_scale.shape
    value_full, gate_full, pool_full = (
        lax.all_gather(value_weight.astype(jnp.bfloat16), "fs", axis=0, tiled=True),
        lax.all_gather(gate_weight.astype(jnp.bfloat16), "fs", axis=0, tiled=True),
        lax.all_gather(pool_weight.astype(jnp.bfloat16), "fs", axis=1, tiled=True),
    )
    down_scales = lax.all_gather(down_scale, "fs", axis=0, tiled=True)
    normed = norm_rows(tokens, mixer_gain).astype(jnp.bfloat16).reshape(row_count, model_width)
    value = jnp.dot(normed, value_full.reshape(model_width, -1), preferred_element_type=jnp.float32)
    value = (
        (value * value_scale.reshape(-1))
        .astype(jnp.bfloat16)
        .reshape(seq_count, seq_length, group_count, local_width)
    )
    gating = jnp.dot(normed, gate_full.reshape(model_width, -1), preferred_element_type=jnp.float32)
    gating = (gating * gate_scale.reshape(-1)).reshape(
        seq_count, seq_length, group_count, local_width
    )
    excess = pool_excess(value).astype(jnp.bfloat16)
    rows_part = pool_full
    pooled = jnp.einsum(
        "slgc,gce->slge",
        lax.all_gather(excess, "tp", axis=3, tiled=True),
        rows_part,
        preferred_element_type=jnp.float32,
    )
    merged = (jax.nn.sigmoid(gating) * (pooled * pool_scale)).astype(jnp.bfloat16)
    merged_own = lax.all_to_all(merged, "tp", split_axis=1, concat_axis=3, tiled=True)
    own_rows = lax.dynamic_slice_in_dim(tokens, member * kept_rows, kept_rows, 1)
    middle = own_rows.reshape(seq_count * kept_rows, model_width).astype(
        jnp.float32
    ) + merged_own.reshape(seq_count * kept_rows, model_width).astype(jnp.float32)
    normed_two = norm_rows(middle, channel_gain).astype(jnp.bfloat16)
    up_full, down_full = (
        lax.all_gather(up_weight.astype(jnp.bfloat16), "fs", axis=0, tiled=True),
        lax.all_gather(down_weight.astype(jnp.bfloat16), "fs", axis=1, tiled=True),
    )
    upward = (
        jnp.dot(
            lax.all_gather(normed_two, "tp", axis=0, tiled=True),
            up_full,
            preferred_element_type=jnp.float32,
        )
        * up_scale
    )
    hidden = jnp.square(jax.nn.relu(upward)).astype(jnp.bfloat16)
    rows_part = hidden
    summed = lax.psum_scatter(
        (jnp.dot(rows_part, down_full, preferred_element_type=jnp.float32) * down_scales).astype(
            jnp.bfloat16
        ),
        "tp",
        scatter_dimension=0,
        tiled=True,
    ).astype(jnp.float32)
    return (middle + summed).astype(jnp.bfloat16).reshape(seq_count, kept_rows, model_width)


def paired_device(
    sizes,
    tokens,
    mixer_gain,
    value_weight,
    value_scale,
    gate_weight,
    gate_scale,
    pool_weight,
    pool_scale,
    channel_gain,
    up_weight,
    up_scale,
    down_weight,
    down_scale,
):
    row = lambda vector: vector.reshape(1, -1)
    out = run_layer(
        sizes,
        (row(mixer_gain), value_scale, gate_scale, pool_scale, row(channel_gain), row(up_scale), row(down_scale)),
        (tokens[0], value_weight, gate_weight, pool_weight, up_weight, down_weight),
    )
    return out[None]


def solution(mesh):
    sizes = dict(mesh.shape)
    paired = sizes["rep"] == 2 and sizes["tp"] == 2 and sizes["fs"] == 8

    def body(tokens, *rest):
        value_scale, down_scale = rest[2], rest[-1]
        square = value_scale.shape[1] == down_scale.shape[0] == rest[1].shape[0]
        if paired and tokens.shape[0] == 1 and square and value_scale.shape[0] == 4:
            return paired_device(sizes, tokens, *rest)
        return per_device(tokens, *rest)

    return jax.shard_map(
        body,
        mesh=mesh,
        in_specs=(
            P(("rep", "fs"), None, None),
            P(),
            P("fs", None, "tp"),
            P(None, "tp"),
            P("fs", None, "tp"),
            P(None, "tp"),
            P(None, "fs", "tp"),
            P(None, "tp"),
            P(),
            P("fs", "tp"),
            P("tp"),
            P("tp", "fs"),
            P("fs"),
        ),
        out_specs=P(("rep", "fs"), "tp", None),
        check_vma=False,
    )
```

time: 203 us -> 185 us (0.911)
  Pallas kernels: 191 us -> 182 us
  other arithmetic: 5.39 us -> 0 us
  local copies, waits for them, and re-layouts: 5.9 us -> 2.73 us
    pallas_call x1, Pallas kernels: 191 us -> 182 us  [run_layer(): pl.pallas_call(functools.partial(layer_kernel, sizes), out_shape=jax.Shap...]
    convert_element_type x5 -> x0, other arithmetic: 5.39 us -> none  [the longest x1 1.62 us: paired_device(): pool_weight.astype(jnp.bfloat16)]
    unnamed x9 -> x1, local copies, waits for them, and re-layouts: 4.54 us -> 2.73 us
where the time goes in v1:
time: 185 us; the launch traced here: 184 us
  Pallas kernels  182 us (98%)
  local copies, waits for them, and re-layouts  2.73 us (1%)
    pallas_call x1, Pallas kernels, run_layer(): pl.pallas_call(functools.partial(layer_kernel, sizes), out_shape=jax.Shap...  182 us

profile of v1, /device:TPU:0, one launch (start us, length us, event | category | flops | bytes accessed | tf_op | source)
XLA Modules:
  0.0 184.4 jit_solution(14938230420200361295)
XLA Ops:
  0.0 181.6 %shard_map.127 = bf16[384,2048]{1,0:T(8,128)(2,1)} custom-call(f32[1,2048]{1,0:T(1,128)} %bitcast.8, f32[4,256]{1,0:T(4,128)} %refs_1_.1, f32[4,256]{1,0:T(4,128)} %refs_2_.1, f32[4,256]{1,0:T(4,128)} %refs_3_.1, f32[1,2048]{1,0:T(1,128)} %bitcast.9, f32[1,2048]{1,0:T(1,128)} %bitcast.10, f32[1,256]{1,0:T(1,128)} %bitcast.11, bf16[768,2048]{1,0:T(8,128)(2,1)} %bitcast.7, ...), custom_call_target="tpu_custom_call" | custom-call | tf_op jit(solution)/shard_map/pallas_call | solution.py:497
  181.6 2.7 %copy.15 = bf16[1,384,2048]{2,1,0:T(8,128)(2,1)} copy(bf16[1,384,2048]{2,1,0:T(8,128)(2,1)} %bitcast.6) | data formatting | bytes 3145728

commit v2 on v1

--- a/solution.py
+++ b/solution.py
@@ -86,10 +86,12 @@
         pl.semaphore_wait(pltpu.get_barrier_semaphore(), 3 + ends)
 
     def each(self, phase, body):
-        if phase < self.nm + self.nh:
-            body(phase)
+        first = 2 * phase
+        if first < self.nm + self.nh:
+            for p in (first, first + 1):
+                body(p)
         else:
-            pl.loop(0, self.subs)(lambda sub: body(self.nm + self.nh + sub))
+            pl.loop(0, self.subs)(lambda sub: body(first + sub))
 
     def source(self, p):
         if not (isinstance(p, int) and p < self.nm and p % 2 == 0):
@@ -98,18 +100,27 @@
         rows = pl.ds(pl.multiple_of(self.rep * part, 16), part)
         return self.stage.at[2 * self.tp + p // 2, rows, :]
 
-    def own(self, phase):
-        def body(p):
+    def own_in(self, *pieces):
+        for p in pieces:
             src = self.source(p)
-
-            @pl.loop(0, 2)
-            def _(way):
-                there = self.inside(self.z + 2 * way - 1)
-                pl.when(there)(lambda: self.copy(p, self.place, way, src=src).start())
+            way = (self.z == 0).astype(jnp.int32)
+            end = (self.z == 0) | (self.z == self.nz - 1)
+            pl.when(end)(lambda: self.copy(p, self.place, way, src=src).start())
+
+    def own_out(self, *pieces):
+        for p in pieces:
+            src = self.source(p)
+
+            @pl.when((self.z > 0) & (self.z < self.nz - 1))
+            def _():
+                for way in range(2):
+                    self.copy(p, self.place, way, src=src).start()
 
             self.copy(p, self.place, ACROSS, src=src).start()
 
-        self.each(phase, body)
+    def own(self, *pieces):
+        self.own_in(*pieces)
+        self.own_out(*pieces)
 
     def along(self, phase, d):
         @pl.loop(0, 2)
@@ -129,43 +140,41 @@
 
                 self.each(phase, body)
 
-    def across(self, phase, d):
-        if d == 0:
-            k = self.z * NY + 1 - self.y
-            way = (self.z == 0).astype(jnp.int32)
-
-            def first(p):
-                self.copy(p, k, ACROSS).wait_recv()
-                pl.when(self.wide(p, self.z))(lambda: self.copy(p, k, way).start())
-                self.copy(p, k, SIBLING).start()
-
-            self.each(phase, first)
-            return
-
+    def facing(self, phase):
+        k = self.z * NY + 1 - self.y
+        way = (self.z == 0).astype(jnp.int32)
+
+        def body(p):
+            self.copy(p, k, ACROSS).wait_recv()
+            pl.when(self.wide(p, self.z))(lambda: self.copy(p, k, way).start())
+            self.copy(p, k, SIBLING).start()
+
+        self.each(phase, body)
+
+    def across(self, phase, d, wide):
         @pl.loop(0, 2)
         def _(way):
             step = 2 * way - 1
             zs = self.z - step * d
-
-            @pl.when(self.inside(zs))
-            def _():
-                k = zs * NY + 1 - self.y
-
-                def body(p):
+            k = zs * NY + 1 - self.y
+
+            def body(p):
+                @pl.when(self.wide(p, zs) if wide else jnp.logical_not(self.wide(p, zs)))
+                def _():
                     self.copy(p, k, ACROSS).wait_recv()
-                    onward = self.wide(p, zs) & self.inside(self.z + step)
-                    pl.when(onward)(lambda: self.copy(p, k, way).start())
+                    if wide:
+                        pl.when(self.inside(self.z + step))(lambda: self.copy(p, k, way).start())
                     self.copy(p, k, SIBLING).start()
 
-                self.each(phase, body)
+            pl.when(self.inside(zs))(lambda: self.each(phase, body))
 
     def wait_sibling(self, phase, k):
         self.each(phase, lambda p: self.copy(p, k, SIBLING, half=1 - self.rep).wait_recv())
 
-    def ready(self, phase):
+    def ready(self, p):
         @pl.loop(0, self.nf)
         def _(k):
-            pl.when(k != self.place)(lambda: self.wait_sibling(phase, k))
+            pl.when(k != self.place)(lambda: self.copy(p, k, SIBLING, half=1 - self.rep).wait_recv())
 
     def drain(self, phase):
         def body(p):
@@ -356,7 +365,7 @@
         if d == 0:
             k = g.z * NY + column
             if column is not g.y:
-                g.wait_sibling(last, k)
+                g.wait_sibling(last // 2, k)
             down_step(k)
             return
 
@@ -367,18 +376,21 @@
             @pl.when(g.inside(zs))
             def _():
                 k = zs * NY + column
-                g.wait_sibling(last, k)
+                g.wait_sibling(last // 2, k)
                 down_step(k)
 
-    def finish():
+    def finish(k):
         wide = show.shape[2]
-
-        @pl.loop(0, g.nf)
-        def _(k):
-            part_copy(k).wait_recv()
-            cut = pl.ds(pl.multiple_of(k * wide, wide), wide)
-            summed = part_own[k].astype(jnp.float32) + part_in[k].astype(jnp.float32)
-            out[:, cut] = (middle_of(k) + summed).astype(out.dtype)
+        part_copy(k).wait_recv()
+        cut = pl.ds(pl.multiple_of(k * wide, wide), wide)
+        summed = part_own[k].astype(jnp.float32) + part_in[k].astype(jnp.float32)
+        out[:, cut] = (middle_of(k) + summed).astype(out.dtype)
+
+    def finish_at(d, column):
+        @pl.loop(0, 1 if d == 0 else 2)
+        def _(way):
+            zs = g.z - (2 * way - 1) * d
+            pl.when(g.inside(zs))(lambda: finish(zs * NY + column))
 
     def middle_of(k):
         owner, slab = k // nm, k % nm
@@ -407,77 +419,128 @@
     g.meet()
     swap(0, rep).start()
     g.own(0)
-    keep(0).start()
+    g.own(2)
+    for j in range(each_group):
+        keep(j).start()
+    swap(0, rep).wait_recv()
+    g.own(1)
     swap(1, rep).start()
-    keep(1).start()
-    swap(0, 1 - rep).start()
-    swap(1, 1 - rep).start()
-    loads[3].wait()
+    for j in range(each_group):
+        swap(j, 1 - rep).start()
+
+    def mix(j):
+        keep(j).wait()
+        swap(j, 1 - rep).wait_recv()
+        for q in range(2):
+            g.ready(2 * j + q)
+            add(value_piece, j, q)
+        for q in range(2):
+            add(gate_piece, j, q)
+
+    def lift(c):
+        g.ready(nm + c)
+        for i in range(hide.shape[3] // local):
+            add(up_piece, c, i)
+
+    def load_up():
+        loads[4].wait()
+        for c in range(nh):
+            round_up(c)
+
+    def load_down():
+        loads[5].wait()
+        for i in range(4):
+            round_down(i)
+
+    show_pieces = tuple(range(last, g.count))
+    inward = ((4, 5), (6, 7), show_pieces, ())
+    outward = ((3,), (4, 5), (6, 7), show_pieces)
+
+    def next_own(phase):
+        g.own_out(*outward[phase])
+        g.own_in(*inward[phase])
+
+    other, show_phase = 1 - g.y, last // 2
+    add(load_up)
+    add(loads[3].wait)
     for i in range(4):
         add(norm_in, i, 4)
-    for load in loads[4:]:
-        add(load.wait)
-    for c in range(nh):
-        add(round_up, c)
-    for i in range(4):
-        add(round_down, i)
-    other, pending = 1 - g.y, []
-    for phase in range(last + 1):
+    add(load_down)
+    emits = ((3, 1, 1, 1, 1, 0, 0, 2), (1, 1, 0, 0, 0, 0, 0, 2), (1, 1, 1, 0, 0, 0, 0, 0), (0, 1, 1, 3, 2, 1, 0, 0))
+    far = g.nz - 1
+    for phase in range(show_phase):
+        counts = emits[phase]
+        if phase == show_phase - 1:
+            for i in range(4):
+                add(norm_mid, i, 4)
         g.along(phase, 1)
-        g.across(phase, 0)
-        if phase + 1 <= last:
-            follow = phase + 1
-            if follow < nm and follow % 2 == 1:
-                swap(follow // 2, rep).wait_recv()
-            g.own(follow)
-        if phase:
-            if phase - 1 < nm and phase % 2 == 0:
-                j = (phase - 1) // 2
-                keep(j).wait()
-                swap(j, 1 - rep).wait_recv()
-                g.ready(phase - 2)
-                g.ready(phase - 1)
-                for q in range(2):
-                    add(value_piece, j, q)
-                for q in range(2):
-                    add(gate_piece, j, q)
-            if phase == last - 2:
-                for i in range(4):
-                    add(norm_mid, i, 4)
-            if phase > nm:
-                g.ready(phase - 1)
-                pending.append(phase - 1 - nm)
-            while phase >= last - 2 and pending:
-                c = pending.pop(0)
-                for i in range(hide.shape[3] // local):
-                    add(up_piece, c, i)
-        if phase >= 2:
-            add(g.drain, phase - 2)
-        if phase == last:
-            add(down_at, 0, g.y)
-            add(down_at, 0, other)
-            add(down_at, 1, g.y)
-        emit(2)
-        for d in range(2, g.nz):
-            g.along(phase, d)
-            g.across(phase, d - 1)
-            if phase == last:
-                add(down_at, d, g.y)
-                add(down_at, d - 1, other)
-            emit(3)
-        if phase == last:
-            add(g.drain, last - 1)
-        g.across(phase, g.nz - 1)
-        emit(3)
+        if phase == 0:
+            swap(1, rep).wait_recv()
+            g.own_in(3)
+        emit(counts[0])
+        g.facing(phase)
+        emit(counts[1])
+        g.along(phase, 2)
+        g.across(phase, 1, True)
+        emit(counts[2])
+        g.along(phase, 3)
+        g.across(phase, 2, True)
+        next_own(phase)
+        if phase == show_phase - 1:
+            for c in range(nh - 2):
+                lift(c)
+        emit(counts[3])
+        g.across(phase, 1, False)
+        emit(counts[4])
+        g.across(phase, 2, False)
+        emit(counts[5])
+        g.across(phase, 3, True)
+        emit(counts[6])
+        g.across(phase, 3, False)
+        if phase < each_group:
+            mix(phase)
+        emit(counts[7])
+        if phase == 1:
+            add(g.drain, 0)
+        elif phase == 2:
+            g.drain(1)
+    lift(nh - 2)
+    lift(nh - 1)
+    add(down_at, 0, g.y)
     emit(len(work))
-    down_at(g.nz - 1, other)
-    for j in range(2):
+    g.along(show_phase, 1)
+    down_at(1, g.y)
+    g.facing(show_phase)
+    down_at(0, other)
+    g.drain(2)
+    g.along(show_phase, 2)
+    g.across(show_phase, 1, True)
+    down_at(2, g.y)
+    g.drain(3)
+    g.across(show_phase, 1, False)
+    down_at(1, other)
+    g.along(show_phase, 3)
+    g.across(show_phase, 2, True)
+    finish_at(0, g.y)
+    down_at(3, g.y)
+    g.across(show_phase, 2, False)
+    down_at(2, other)
+    finish_at(1, g.y)
+    finish_at(0, other)
+    g.across(show_phase, 3, True)
+    g.across(show_phase, 3, False)
+    down_at(3, other)
+    finish_at(2, g.y)
+    finish_at(1, other)
+    for j in range(each_group):
         for part in range(2):
             swap(j, part).wait_send()
     for slab in range(nm):
         merged_copy(slab).wait_send()
-    g.drain(last)
-    finish()
+    g.drain(show_phase)
+    finish_at(far, g.y)
+    finish_at(2, other)
+    finish_at(far, other)
 
     @pl.loop(0, g.nf)
     def _(k):
@@ -494,8 +557,19 @@
     vmem = lambda dims, kind=jnp.bfloat16: pltpu.VMEM(tuple(dims), kind)
     halves = (nf, rows // 2, wide)
     count = 12
+    sems = [
+        pltpu.SemaphoreType.DMA((4, count, nf)),
+        pltpu.SemaphoreType.DMA((2, count, nf)),
+        pltpu.SemaphoreType.DMA((len(arrays),)),
+        pltpu.SemaphoreType.DMA((2, 2)),
+        pltpu.SemaphoreType.DMA((2, 2)),
+        pltpu.SemaphoreType.DMA((2,)),
+        pltpu.SemaphoreType.DMA((2, nf)),
+        pltpu.SemaphoreType.DMA((2, nf)),
+    ]
+    kernel = lambda *refs: pl.run_scoped(functools.partial(layer_kernel, sizes, *refs), *sems)
     return pl.pallas_call(
-        functools.partial(layer_kernel, sizes),
+        kernel,
         out_shape=jax.ShapeDtypeStruct((rows // 2, width), jnp.bfloat16),
         in_specs=[pl.BlockSpec(memory_space=pltpu.VMEM)] * len(vectors)
         + [pl.BlockSpec(memory_space=pl.ANY)] * len(arrays),
@@ -517,14 +591,6 @@
             vmem(halves),
             vmem(halves),
             vmem(halves),
-            pltpu.SemaphoreType.DMA((4, count, nf)),
-            pltpu.SemaphoreType.DMA((2, count, nf)),
-            pltpu.SemaphoreType.DMA((len(arrays),)),
-            pltpu.SemaphoreType.DMA((2, 2)),
-            pltpu.SemaphoreType.DMA((2, 2)),
-            pltpu.SemaphoreType.DMA((2,)),
-            pltpu.SemaphoreType.DMA((2, nf)),
-            pltpu.SemaphoreType.DMA((2, nf)),
         ],
         compiler_params=pltpu.CompilerParams(
             collective_id=0, has_side_effects=True, vmem_limit_bytes=63 * 2**20

time: 185 us -> 153 us (0.83)
  Pallas kernels: 182 us -> 150 us
    pallas_call x1, Pallas kernels: 182 us -> 150 us  [run_layer(): pl.pallas_call(kernel, out_shape=jax.ShapeDtypeStruct((rows // 2, width),...]
where the time goes in v2:
time: 153 us
  Pallas kernels  150 us (98%)
  local copies, waits for them, and re-layouts  2.73 us (2%)
    pallas_call x1, Pallas kernels, run_layer(): pl.pallas_call(kernel, out_shape=jax.ShapeDtypeStruct((rows // 2, width),...  150 us

profile of v2, /device:TPU:0, one launch (start us, length us, event | category | flops | bytes accessed | tf_op | source)
XLA Modules:
  0.0 153.1 jit_solution(2373864965413562374)
XLA Ops:
  0.0 150.4 %shard_map.127 = bf16[384,2048]{1,0:T(8,128)(2,1)} custom-call(f32[1,2048]{1,0:T(1,128)} %bitcast.8, f32[4,256]{1,0:T(4,128)} %refs_1_.1, f32[4,256]{1,0:T(4,128)} %refs_2_.1, f32[4,256]{1,0:T(4,128)} %refs_3_.1, f32[1,2048]{1,0:T(1,128)} %bitcast.9, f32[1,2048]{1,0:T(1,128)} %bitcast.10, f32[1,256]{1,0:T(1,128)} %bitcast.11, bf16[768,2048]{1,0:T(8,128)(2,1)} %bitcast.7, ...), custom_call_target="tpu_custom_call" | custom-call | tf_op jit(solution)/shard_map/pallas_call | solution.py:571
  150.4 2.7 %copy.15 = bf16[1,384,2048]{2,1,0:T(8,128)(2,1)} copy(bf16[1,384,2048]{2,1,0:T(8,128)(2,1)} %bitcast.6) | data formatting | bytes 3145728

commit v3 on v2

--- a/solution.py
+++ b/solution.py
@@ -41,15 +41,15 @@
         return 2 * j + (self.tp if q == 0 else 1 - self.tp)
 
     def piece(self, p, k, half):
-        if isinstance(p, int) and p < self.nm:
+        if p < self.nm:
             part = self.mixed.shape[2] // 2
             return self.mixed.at[self.half_of(p), k, pl.ds(pl.multiple_of(half * part, 16), part), :]
-        if isinstance(p, int) and p < self.nm + self.nh:
+        if p < self.nm + self.nh:
             part = self.hide.shape[2] // 2
             return self.hide.at[p - self.nm, k, pl.ds(pl.multiple_of(half * part, 16), part), :]
-        part = self.show.shape[1] // (2 * self.subs)
-        sub = p - self.nm - self.nh
-        return self.show.at[k, pl.ds(pl.multiple_of((2 * sub + half) * part, 16), part), :]
+        part = self.show.shape[2] // 4
+        side, deep = (p - self.nm - self.nh) // 2, p % 2
+        return self.show.at[k, side, pl.ds(pl.multiple_of((2 * deep + half) * part, 16), part), :]
 
     def copy(self, p, k, way, half=None, src=None):
         half = self.rep if half is None else half
@@ -86,15 +86,11 @@
         pl.semaphore_wait(pltpu.get_barrier_semaphore(), 3 + ends)
 
     def each(self, phase, body):
-        first = 2 * phase
-        if first < self.nm + self.nh:
-            for p in (first, first + 1):
-                body(p)
-        else:
-            pl.loop(0, self.subs)(lambda sub: body(first + sub))
+        for p in (2 * phase, 2 * phase + 1):
+            body(p)
 
     def source(self, p):
-        if not (isinstance(p, int) and p < self.nm and p % 2 == 0):
+        if p >= self.nm or p % 2:
             return None
         part = self.stage.shape[1] // 2
         rows = pl.ds(pl.multiple_of(self.rep * part, 16), part)
@@ -204,17 +200,18 @@
     tokens_far, value_far, gate_far, pool_far, up_far, down_far, out = refs[7:14]
     mixed, hide, show, stage = refs[14:18]
     tokens, value_near, gate_near, pool_near, up_near, down_near = refs[18:24]
-    normed, excess, merged, merged_in, hidden, part_out, part_own, part_in = refs[24:32]
-    send_sem, recv_sem, load_sem, swap_send, swap_recv, keep_sem, pair_send, pair_recv = refs[32:]
+    normed, excess, merged, merged_in, hidden, parts, part_in = refs[24:31]
+    send_sem, recv_sem, load_sem, swap_send, swap_recv, keep_sem, pair_send, pair_recv, part_send, part_recv = refs[31:]
     g = Gather(sizes, (mixed, hide, show, stage), (send_sem, recv_sem))
     rows, width = tokens.shape
     groups, cells, local = pool_near.shape
     depth = value_near.shape[0]
-    half = rows // 2
+    half, block = rows // 2, rows // 12
     inner = hidden.shape[1]
     member, rep, place = g.tp, g.rep, g.place
     nm, nh = g.nm, g.nh
     last = nm + nh
+    show_phase = last // 2
     each_group = nm // 2
 
     loads = [
@@ -255,10 +252,10 @@
         return pltpu.make_async_copy(stage.at[2 * member + j], mixed.at[2 * j + member, place], keep_sem.at[j])
 
     def merged_copy(slab):
-        return remote(merged.at[slab], merged_in.at[slab], pair_send.at[0, slab], pair_recv.at[0, slab])
-
-    def part_copy(k):
-        return remote(part_out.at[k], part_in.at[k], pair_send.at[1, k], pair_recv.at[1, k])
+        return remote(merged.at[slab], merged_in.at[slab], pair_send.at[slab], pair_recv.at[slab])
+
+    def part_copy(k, c):
+        return remote(parts.at[0, k, c], part_in.at[k, c], part_send.at[k, c], part_recv.at[k, c])
 
     def round_mixed(group):
         stage[group, :depth, :local] = (value_near[:, group, :] * value_scale[group : group + 1]).astype(jnp.bfloat16)
@@ -275,14 +272,17 @@
     def round_down(i):
         part = inner // 4
         at = pl.ds(i * part, part)
-        show[place, at, :] = (down_near[at, :] * down_scale[...]).astype(jnp.bfloat16)
+        side = show.shape[3]
+        for c in range(2):
+            cut = slice(c * side, (c + 1) * side)
+            show[place, c, at, :] = (down_near[at, cut] * down_scale[:, cut]).astype(jnp.bfloat16)
 
     def norm_in(part, parts):
-        steps = rows // 16 // parts
+        steps = rows // block // parts
 
         @pl.loop(part * steps, (part + 1) * steps)
         def _(i):
-            at = pl.ds(pl.multiple_of(i * 16, 16), 16)
+            at = pl.ds(pl.multiple_of(i * block, block), block)
             normed[at, :] = norm_rows(tokens[at, :], mixer_gain[...]).astype(jnp.bfloat16)
 
     def slab_of(j, q):
@@ -291,20 +291,33 @@
     def value_piece(j, q):
         slab = slab_of(j, q)
         weight = mixed[slab, :, :depth, :local].reshape(width, local)
-        value = jnp.dot(normed[...], weight, preferred_element_type=jnp.float32)
-        floats = value.astype(jnp.bfloat16).astype(jnp.float32)
-        position = lax.broadcasted_iota(jnp.int32, floats.shape, 0)
+
+        @pl.loop(0, 2)
+        def _(i):
+            at = pl.ds(pl.multiple_of(i * half, half), half)
+            value = jnp.dot(normed[at, :], weight, preferred_element_type=jnp.float32)
+            excess[slab - 2 * j, at, :] = value.astype(jnp.bfloat16)
+
+    def spread_piece(j, q):
+        slab = slab_of(j, q)
         group = each_group * member + j
-        running = floats
-        for level in range(groups - each_group + j + 1):
-            shifted = pltpu.roll(running, 2**level, 0)
-            start = jnp.where(level <= group, 2**level, rows)
-            running = running + jnp.where(position >= start, shifted, 0.0)
         window = jnp.int32(2)
         for level in range(groups - 1):
             window = jnp.where(group > level, 2 ** (level + 2), window)
-        counts = jnp.minimum(position + 1, window).astype(jnp.float32)
-        excess[slab - 2 * j] = (running / counts - floats).astype(jnp.bfloat16)
+        lanes = local // 2
+
+        @pl.loop(0, 2)
+        def _(i):
+            cut = pl.ds(pl.multiple_of(i * lanes, lanes), lanes)
+            floats = excess[slab - 2 * j, :, cut].astype(jnp.float32)
+            position = lax.broadcasted_iota(jnp.int32, floats.shape, 0)
+            running = floats
+            for level in range(groups - each_group + j + 1):
+                shifted = pltpu.roll(running, 2**level, 0)
+                start = jnp.where(level <= group, 2**level, rows)
+                running = running + jnp.where(position >= start, shifted, 0.0)
+            counts = jnp.minimum(position + 1, window).astype(jnp.float32)
+            excess[slab - 2 * j, :, cut] = (running / counts - floats).astype(jnp.bfloat16)
 
     def gate_piece(j, q):
         slab = slab_of(j, q)
@@ -327,11 +340,11 @@
         if part == 0:
             for slab in range(nm):
                 merged_copy(slab).wait_recv()
-        steps = rows // 16 // parts
+        steps = rows // block // parts
 
         @pl.loop(part * steps, (part + 1) * steps)
         def _(i):
-            at = pl.ds(pl.multiple_of(i * 16, 16), 16)
+            at = pl.ds(pl.multiple_of(i * block, block), block)
             held = []
             for slab in range(nm):
                 for source, owner in ((merged, member), (merged_in, 1 - member)):
@@ -352,21 +365,21 @@
             upward = jnp.dot(normed[at, :], weight, preferred_element_type=jnp.float32)
             hidden[at, first : first + local] = jnp.square(jax.nn.relu(upward)).astype(jnp.bfloat16)
 
-    def down_half(k, first):
-        at = pl.ds(pl.multiple_of(first, half), half)
-        return jnp.dot(hidden[at, :], show[k], preferred_element_type=jnp.float32).astype(jnp.bfloat16)
-
-    def down_step(k):
-        part_out[k] = down_half(k, (1 - member) * half)
-        part_copy(k).start()
-        part_own[k] = down_half(k, member * half)
-
-    def down_at(d, column):
+    def down_step(k, c):
+        @pl.loop(0, 2)
+        def _(b):
+            first = lax.rem(b + member + 1, 2) * half
+            at = pl.ds(pl.multiple_of(first, half), half)
+            part = jnp.dot(hidden[at, :], show[k, c], preferred_element_type=jnp.float32)
+            parts[b, k, c] = part.astype(jnp.bfloat16)
+            pl.when(b == 0)(lambda: part_copy(k, c).start())
+
+    def down_at(d, column, c):
         if d == 0:
             k = g.z * NY + column
             if column is not g.y:
-                g.wait_sibling(last // 2, k)
-            down_step(k)
+                g.wait_sibling(show_phase + c, k)
+            down_step(k, c)
             return
 
         @pl.loop(0, 2)
@@ -376,15 +389,16 @@
             @pl.when(g.inside(zs))
             def _():
                 k = zs * NY + column
-                g.wait_sibling(last // 2, k)
-                down_step(k)
+                g.wait_sibling(show_phase + c, k)
+                down_step(k, c)
 
     def finish(k):
-        wide = show.shape[2]
-        part_copy(k).wait_recv()
-        cut = pl.ds(pl.multiple_of(k * wide, wide), wide)
-        summed = part_own[k].astype(jnp.float32) + part_in[k].astype(jnp.float32)
-        out[:, cut] = (middle_of(k) + summed).astype(out.dtype)
+        side = show.shape[3]
+        for c in range(2):
+            part_copy(k, c).wait_recv()
+            cut = pl.ds(pl.multiple_of((2 * k + c) * side, side), side)
+            summed = parts[1, k, c].astype(jnp.float32) + part_in[k, c].astype(jnp.float32)
+            out[:, cut] = (middle_of(k, c) + summed).astype(out.dtype)
 
     def finish_at(d, column):
         @pl.loop(0, 1 if d == 0 else 2)
@@ -392,12 +406,14 @@
             zs = g.z - (2 * way - 1) * d
             pl.when(g.inside(zs))(lambda: finish(zs * NY + column))
 
-    def middle_of(k):
+    def middle_of(k, c):
         owner, slab = k // nm, k % nm
-        cut = pl.ds(pl.multiple_of(k * local, local), local)
+        side = show.shape[3]
+        cut = pl.ds(pl.multiple_of((2 * k + c) * side, side), side)
         at = pl.ds(pl.multiple_of(member * half, half), half)
-        own = merged[slab, at, :].astype(jnp.float32)
-        theirs = merged_in[slab, at, :].astype(jnp.float32)
+        near = slice(c * side, (c + 1) * side)
+        own = merged[slab, at, near].astype(jnp.float32)
+        theirs = merged_in[slab, at, near].astype(jnp.float32)
         return tokens[at, cut].astype(jnp.float32) + jnp.where(owner == member, own, theirs)
 
     work = []
@@ -434,6 +450,7 @@
         for q in range(2):
             g.ready(2 * j + q)
             add(value_piece, j, q)
+            add(spread_piece, j, q)
         for q in range(2):
             add(gate_piece, j, q)
 
@@ -454,19 +471,19 @@
 
     show_pieces = tuple(range(last, g.count))
     inward = ((4, 5), (6, 7), show_pieces, ())
-    outward = ((3,), (4, 5), (6, 7), show_pieces)
+    outward = ((3, 4), (5, 6), (7,), show_pieces)
 
     def next_own(phase):
         g.own_out(*outward[phase])
         g.own_in(*inward[phase])
 
-    other, show_phase = 1 - g.y, last // 2
+    other = 1 - g.y
     add(load_up)
     add(loads[3].wait)
     for i in range(4):
         add(norm_in, i, 4)
     add(load_down)
-    emits = ((3, 1, 1, 1, 1, 0, 0, 2), (1, 1, 0, 0, 0, 0, 0, 2), (1, 1, 1, 0, 0, 0, 0, 0), (0, 1, 1, 3, 2, 1, 0, 0))
+    emits = ((3, 1, 1, 1, 1, 0, 0, 2), (2, 1, 1, 0, 0, 0, 0, 2), (2, 1, 1, 0, 0, 0, 0, 0), (0, 2, 2, 2, 1, 1, 0, 0))
     far = g.nz - 1
     for phase in range(show_phase):
         counts = emits[phase]
@@ -504,47 +521,70 @@
             add(g.drain, 0)
         elif phase == 2:
             g.drain(1)
+    first, second = show_phase, show_phase + 1
     lift(nh - 2)
     lift(nh - 1)
-    add(down_at, 0, g.y)
+    emit(len(work) - 4)
+    g.along(first, 1)
+    emit(len(work) - 1)
+    g.along(second, 1)
     emit(len(work))
-    g.along(show_phase, 1)
-    down_at(1, g.y)
-    g.facing(show_phase)
-    down_at(0, other)
+    g.facing(first)
+    down_at(0, g.y, 0)
+    down_at(0, g.y, 1)
+    g.facing(second)
     g.drain(2)
-    g.along(show_phase, 2)
-    g.across(show_phase, 1, True)
-    down_at(2, g.y)
+    down_at(1, g.y, 0)
+    g.along(first, 2)
+    g.across(first, 1, True)
+    down_at(0, other, 0)
+    down_at(1, g.y, 1)
     g.drain(3)
-    g.across(show_phase, 1, False)
-    down_at(1, other)
-    g.along(show_phase, 3)
-    g.across(show_phase, 2, True)
+    down_at(0, other, 1)
+    g.across(first, 1, False)
+    down_at(2, g.y, 0)
+    g.along(second, 2)
+    g.across(second, 1, True)
+    down_at(1, other, 0)
+    g.across(second, 1, False)
+    down_at(2, g.y, 1)
+    g.along(first, 3)
+    g.across(first, 2, True)
+    down_at(1, other, 1)
+    g.across(first, 2, False)
+    down_at(3, g.y, 0)
+    g.along(second, 3)
+    g.across(second, 2, True)
+    down_at(2, other, 0)
     finish_at(0, g.y)
-    down_at(3, g.y)
-    g.across(show_phase, 2, False)
-    down_at(2, other)
+    g.across(second, 2, False)
+    down_at(3, g.y, 1)
     finish_at(1, g.y)
+    g.across(first, 3, True)
+    g.across(first, 3, False)
+    down_at(2, other, 1)
     finish_at(0, other)
-    g.across(show_phase, 3, True)
-    g.across(show_phase, 3, False)
-    down_at(3, other)
+    g.across(second, 3, True)
+    g.across(second, 3, False)
+    down_at(3, other, 0)
+    down_at(3, other, 1)
     finish_at(2, g.y)
     finish_at(1, other)
+    g.drain(first)
     for j in range(each_group):
         for part in range(2):
             swap(j, part).wait_send()
     for slab in range(nm):
         merged_copy(slab).wait_send()
-    g.drain(show_phase)
+    g.drain(second)
     finish_at(far, g.y)
     finish_at(2, other)
     finish_at(far, other)
 
     @pl.loop(0, g.nf)
     def _(k):
-        part_copy(k).wait_send()
+        for c in range(2):
+            part_copy(k, c).wait_send()
 
 
 def run_layer(sizes, vectors, arrays):
@@ -555,7 +595,7 @@
     inner, wide = down.shape
     nf = sizes["fs"]
     vmem = lambda dims, kind=jnp.bfloat16: pltpu.VMEM(tuple(dims), kind)
-    halves = (nf, rows // 2, wide)
+    halves = (nf, 2, rows // 2, wide // 2)
     count = 12
     sems = [
         pltpu.SemaphoreType.DMA((4, count, nf)),
@@ -564,20 +604,22 @@
         pltpu.SemaphoreType.DMA((2, 2)),
         pltpu.SemaphoreType.DMA((2, 2)),
         pltpu.SemaphoreType.DMA((2,)),
-        pltpu.SemaphoreType.DMA((2, nf)),
-        pltpu.SemaphoreType.DMA((2, nf)),
+        pltpu.SemaphoreType.DMA((groups,)),
+        pltpu.SemaphoreType.DMA((groups,)),
+        pltpu.SemaphoreType.DMA((nf, 2)),
+        pltpu.SemaphoreType.DMA((nf, 2)),
     ]
     kernel = lambda *refs: pl.run_scoped(functools.partial(layer_kernel, sizes, *refs), *sems)
     return pl.pallas_call(
         kernel,
-        out_shape=jax.ShapeDtypeStruct((rows // 2, width), jnp.bfloat16),
+        out_shape=pltpu.VMEM((rows // 2, width), jnp.bfloat16),
         in_specs=[pl.BlockSpec(memory_space=pltpu.VMEM)] * len(vectors)
         + [pl.BlockSpec(memory_space=pl.ANY)] * len(arrays),
         out_specs=pl.BlockSpec(memory_space=pltpu.VMEM),
         scratch_shapes=[
             vmem((groups, nf, depth + cells // 2, 2 * local)),
             vmem((inner // (2 * local), nf, depth, 2 * local)),
-            vmem((nf, inner, wide)),
+            vmem((nf, 2, inner, wide // 2)),
             vmem((groups, depth + cells // 2, 2 * local)),
             vmem(tokens.shape),
         ]
@@ -588,12 +630,11 @@
             vmem((groups, rows, local)),
             vmem((groups, rows, local)),
             vmem((rows, inner)),
-            vmem(halves),
-            vmem(halves),
+            vmem((2, *halves)),
             vmem(halves),
         ],
         compiler_params=pltpu.CompilerParams(
-            collective_id=0, has_side_effects=True, vmem_limit_bytes=63 * 2**20
+            collective_id=0, has_side_effects=True, vmem_limit_bytes=58 * 2**20
         ),
     )(*vectors, *arrays)
 

time: 153 us -> 146 us (0.954)
  Pallas kernels: 150 us -> 144 us
  local copies, waits for them, and re-layouts: 2.73 us -> 1.15 us
    pallas_call x1, Pallas kernels: 150 us -> 144 us  [run_layer(): pl.pallas_call(kernel, out_shape=pltpu.VMEM((rows // 2, width), jnp.bfloa...]
    unnamed x1, local copies, waits for them, and re-layouts: 2.73 us -> 1.15 us
where the time goes in v3:
time: 146 us; the launch traced here: 145 us
  Pallas kernels  144 us (99%)
    pallas_call x1, Pallas kernels, run_layer(): pl.pallas_call(kernel, out_shape=pltpu.VMEM((rows // 2, width), jnp.bfloa...  144 us

profile of v3, /device:TPU:0, one launch (start us, length us, event | category | flops | bytes accessed | tf_op | source)
XLA Modules:
  0.0 145.4 jit_solution(18400383843837625239)
XLA Ops:
  0.0 144.2 %shard_map.127 = bf16[384,2048]{1,0:T(8,128)(2,1)S(1)} custom-call(f32[1,2048]{1,0:T(1,128)} %bitcast.8, f32[4,256]{1,0:T(4,128)} %refs_1_.1, f32[4,256]{1,0:T(4,128)} %refs_2_.1, f32[4,256]{1,0:T(4,128)} %refs_3_.1, f32[1,2048]{1,0:T(1,128)} %bitcast.9, f32[1,2048]{1,0:T(1,128)} %bitcast.10, f32[1,256]{1,0:T(1,128)} %bitcast.11, bf16[768,2048]{1,0:T(8,128)(2,1)} %bitcast.7, ...), custom_call_target="tpu_custom_call" | custom-call | tf_op jit(solution)/shard_map/pallas_call | solution.py:613
  144.2 1.1 copy.15

commit v4 on v3

--- a/solution.py
+++ b/solution.py
@@ -196,12 +196,13 @@
 
 
 def layer_kernel(sizes, *refs):
-    mixer_gain, value_scale, gate_scale, pool_scale, channel_gain, up_scale, down_scale = refs[:7]
+    vectors_far, vectors = refs[:7], refs[31:38]
+    mixer_gain, value_scale, gate_scale, pool_scale, channel_gain, up_scale, down_scale = vectors
     tokens_far, value_far, gate_far, pool_far, up_far, down_far, out = refs[7:14]
     mixed, hide, show, stage = refs[14:18]
     tokens, value_near, gate_near, pool_near, up_near, down_near = refs[18:24]
     normed, excess, merged, merged_in, hidden, parts, part_in = refs[24:31]
-    send_sem, recv_sem, load_sem, swap_send, swap_recv, keep_sem, pair_send, pair_recv, part_send, part_recv = refs[31:]
+    send_sem, recv_sem, load_sem, swap_send, swap_recv, keep_sem, pair_send, pair_recv, part_send, part_recv = refs[38:]
     g = Gather(sizes, (mixed, hide, show, stage), (send_sem, recv_sem))
     rows, width = tokens.shape
     groups, cells, local = pool_near.shape
@@ -228,6 +229,11 @@
         )
     ]
 
+    small = [
+        pltpu.make_async_copy(far, near, load_sem.at[len(loads) + i])
+        for i, (far, near) in enumerate(zip(vectors_far, vectors))
+    ]
+
     def remote(source, target, send, recv):
         return pltpu.make_async_remote_copy(
             src_ref=source,
@@ -426,9 +432,9 @@
         work.append(functools.partial(function, *args))
 
     g.greet()
-    for load in loads:
+    for load in loads[:3] + small:
         load.start()
-    for load in loads[:3]:
+    for load in loads[:3] + small:
         load.wait()
     for group in range(groups):
         round_mixed(group)
@@ -436,6 +442,8 @@
     swap(0, rep).start()
     g.own(0)
     g.own(2)
+    for load in loads[3:]:
+        load.start()
     for j in range(each_group):
         keep(j).start()
     swap(0, rep).wait_recv()
@@ -600,7 +608,7 @@
     sems = [
         pltpu.SemaphoreType.DMA((4, count, nf)),
         pltpu.SemaphoreType.DMA((2, count, nf)),
-        pltpu.SemaphoreType.DMA((len(arrays),)),
+        pltpu.SemaphoreType.DMA((len(arrays) + len(vectors),)),
         pltpu.SemaphoreType.DMA((2, 2)),
         pltpu.SemaphoreType.DMA((2, 2)),
         pltpu.SemaphoreType.DMA((2,)),
@@ -613,8 +621,7 @@
     return pl.pallas_call(
         kernel,
         out_shape=pltpu.VMEM((rows // 2, width), jnp.bfloat16),
-        in_specs=[pl.BlockSpec(memory_space=pltpu.VMEM)] * len(vectors)
-        + [pl.BlockSpec(memory_space=pl.ANY)] * len(arrays),
+        in_specs=[pl.BlockSpec(memory_space=pl.ANY)] * (len(vectors) + len(arrays)),
         out_specs=pl.BlockSpec(memory_space=pltpu.VMEM),
         scratch_shapes=[
             vmem((groups, nf, depth + cells // 2, 2 * local)),
@@ -632,6 +639,7 @@
             vmem((rows, inner)),
             vmem((2, *halves)),
             vmem(halves),
+            *[vmem(vector.shape, vector.dtype) for vector in vectors],
         ],
         compiler_params=pltpu.CompilerParams(
             collective_id=0, has_side_effects=True, vmem_limit_bytes=58 * 2**20

time: 146 us -> 145 us (level)
  no operation moved by 1% of the time
where the time goes in v4:
time: 145 us
  Pallas kernels  143 us (99%)
    pallas_call x1, Pallas kernels, run_layer(): pl.pallas_call(kernel, out_shape=pltpu.VMEM((rows // 2, width), jnp.bfloa...  143 us

profile of v4, /device:TPU:0, one launch (start us, length us, event | category | flops | bytes accessed | tf_op | source)
XLA Modules:
  0.0 144.6 jit_solution(6670785900373045690)
XLA Ops:
  0.0 143.5 %shard_map.127 = bf16[384,2048]{1,0:T(8,128)(2,1)S(1)} custom-call(f32[1,2048]{1,0:T(1,128)} %bitcast.8, f32[4,256]{1,0:T(4,128)} %refs_1_.1, f32[4,256]{1,0:T(4,128)} %refs_2_.1, f32[4,256]{1,0:T(4,128)} %refs_3_.1, f32[1,2048]{1,0:T(1,128)} %bitcast.9, f32[1,2048]{1,0:T(1,128)} %bitcast.10, f32[1,256]{1,0:T(1,128)} %bitcast.11, bf16[768,2048]{1,0:T(8,128)(2,1)} %bitcast.7, ...), custom_call_target="tpu_custom_call" | custom-call | tf_op jit(solution)/shard_map/pallas_call | solution.py:621
  143.5 1.1 copy.15
